TPU v7x, 128 devices: a whole 4x4x4 slice. The times are simulated.
128 devices in a mesh: sp: 16 (over z, x), fs: 4 (over y), tp: 2 (over core).
Axes of the slice: x: 4, y: 4, z: 4, core: 2. Of those that a mesh axis runs over, the one named last changes fastest.
Arguments:
- tokens: bfloat16 [4, 8192, 2048], P('fs', 'sp', 'tp'), may hold values from -6 to 6
- norm_gain: float32 [2048], replicated, may hold values from 0.1 to 1.9
- w_pool_in: bfloat16 [2048, 512], P('fs', 'tp'), may hold values from -0.125 to 0.125
- w_query: bfloat16 [2048, 1024], P('fs', 'tp'), may hold values from -0.125 to 0.125
- w_key: bfloat16 [2048, 1024], P('fs', 'tp'), may hold values from -0.125 to 0.125
- w_value: bfloat16 [2048, 1024], P('fs', 'tp'), may hold values from -0.125 to 0.125
- query_gain: float32 [64], replicated, may hold values from 1.5 to 2.5
- key_gain: float32 [64], replicated, may hold values from 1.5 to 2.5
- stick_offset: float32 [16], P('tp'), as said below
- pool_mix: bfloat16 [4, 128, 128], P('tp'), may hold values from -0.5 to 0.5
- pool_scale: float32 [512], P('tp'), may hold values from 0.2 to 4, as said below
- pool_gain: bfloat16 [512], P('tp'), may hold values from 0.099609375 to 1.8984375
- attn_gain: bfloat16 [1024], P('tp'), may hold values from 0.099609375 to 1.8984375
- w_out_pool: bfloat16 [512, 2048], P('tp', 'fs'), may hold values from -0.15625 to 0.15625
- w_out_attn: bfloat16 [1024, 2048], P('tp', 'fs'), may hold values from -0.15625 to 0.15625
Outputs:
- mixed: bfloat16 [4, 8192, 2048], P('fs', ('sp', 'tp'))
Inputs may be any that keep to these rules, and one draw needn't show every extreme that they name: `stick_offset`: per head, negative. `pool_scale`: positive channel scales.
All inputs are finite; a program needn't handle non-finite values.
Results may differ from a plain program's by a relative error of at most 0.013.
Values may be sent and summed in bfloat16 or wider, within the bound.
A program may use at most 192 MiB of HBM per device.

v0:
```python
import math
import jax
import jax.numpy as jnp
from jax import lax
from jax.sharding import PartitionSpec as P

HEADS = 16
HEAD_DIM = 64
POOL = 512
POOL_GROUPS = 4
EPS = 1e-06


def sent_to_all(shard, axis):
    devices = lax.axis_size(axis)
    return lax.all_to_all(
        jnp.broadcast_to(shard[None], (devices, *shard.shape)), axis, 0, 0, tiled=True
    )


def in_order(parts, dim):
    lengths = list(parts.shape[1:])
    lengths[dim] *= parts.shape[0]
    return jnp.moveaxis(parts, 0, dim).reshape(lengths)


def gathered_copies(shard, axis, dim):
    parts = sent_to_all(shard, axis)
    return in_order(parts, dim)


def in_one_piece(arrays, axis, dim, along):
    both = jnp.concatenate(arrays, axis=along)
    whole, at, outs = (lax.all_gather(both, axis, axis=dim, tiled=True), 0, [])
    for a in arrays:
        outs.append(lax.slice_in_dim(whole, at, at + a.shape[along], axis=along))
        at += a.shape[along]
    return tuple(outs)


def shifted_2(value, axis, steps):
    count = lax.axis_size(axis)
    initial, last = (max(0, -steps), min(count, count - steps))
    return lax.ppermute(value, axis, [(source, source + steps) for source in range(initial, last)])


def partner_2(shard, axis, distance):
    return lax.ppermute(shard, axis, [(i, i ^ 1 << distance) for i in range(lax.axis_size(axis))])


def head_norm(projected, gain, head_count):
    split = projected.reshape(projected.shape[0], head_count, HEAD_DIM)
    factor = lax.rsqrt(jnp.mean(split * split, axis=-1, keepdims=True) + EPS)
    return (split * factor * gain).astype(jnp.bfloat16)


def stick_block(query, key_heads, value_heads, offset, carried, row_offset, score_scale):
    scores = (
        jnp.einsum("thd,khd->htk", query, key_heads, preferred_element_type=jnp.float32)
        * score_scale
        + offset[:, None, None]
    )
    keep = jax.nn.log_sigmoid(-scores)
    if row_offset is not None:
        shape = (query.shape[0], key_heads.shape[0])
        earlier = (
            lax.broadcasted_iota(jnp.int32, shape, 1)
            < lax.broadcasted_iota(jnp.int32, shape, 0) + row_offset
        )
        keep = jnp.where(earlier[None], keep, 0.0)
    running = jnp.cumsum(keep, axis=2)
    block_total = running[:, :, -1]
    log_weight = (
        jax.nn.log_sigmoid(scores) + block_total[:, :, None] - running + carried[:, :, None]
    )
    weight = jnp.exp(log_weight)
    if row_offset is not None:
        weight = jnp.where(earlier[None], weight, 0.0)
    weight = weight.astype(jnp.bfloat16)
    block_out = jnp.einsum("htk,khd->thd", weight, value_heads, preferred_element_type=jnp.float32)
    return (block_out, block_total)


def branch_norm(values_in, squares, width, gain):
    values_f = values_in.astype(jnp.float32)
    factor = lax.rsqrt(squares / width + EPS)
    return (values_f * factor[:, None] * gain.astype(jnp.float32)).astype(jnp.bfloat16)


def shards(
    tokens,
    norm_gain,
    w_pool_in,
    w_query,
    w_key,
    w_value,
    query_gain,
    key_gain,
    stick_offset,
    pool_mix,
    pool_scale,
    pool_gain,
    attn_gain,
    w_out_pool,
    w_out_attn,
):
    whole = gathered_copies(tokens, "tp", 2)[0]
    whole_f = whole.astype(jnp.float32)
    normed = (
        whole_f * lax.rsqrt(jnp.mean(whole_f * whole_f, axis=-1, keepdims=True) + EPS) * norm_gain
    ).astype(jnp.bfloat16)
    row_count = normed.shape[0]
    pieces = in_one_piece((w_pool_in, w_query, w_key, w_value), "fs", 0, 1)
    pool_raw, query_raw, key_raw, value_raw = tuple(
        (jnp.dot(normed, piece, preferred_element_type=jnp.float32) for piece in pieces)
    )
    head_count = query_raw.shape[1] // HEAD_DIM
    query = head_norm(query_raw, query_gain, head_count)
    key_heads = head_norm(key_raw, key_gain, head_count)
    value_heads = value_raw.astype(jnp.bfloat16).reshape(row_count, head_count, HEAD_DIM)
    reach = 16
    pool_in = pool_raw.astype(jnp.bfloat16)
    previous = shifted_2(pool_in[row_count - reach :], "sp", 1)
    extended = jnp.concatenate([previous, pool_in], axis=0).astype(jnp.float32)
    pool_cols = pool_in.shape[1]
    group_ch = POOL // POOL_GROUPS
    local_groups = pool_cols // group_ch
    group_ids = (
        lax.axis_index("tp") * local_groups + jnp.arange(pool_cols, dtype=jnp.int32) // group_ch
    )
    window = jnp.left_shift(jnp.int32(2), group_ids)
    summed = jnp.zeros((row_count, pool_cols), jnp.float32)
    for behind in range(reach):
        shifted = extended[reach - behind : reach - behind + row_count]
        summed = summed + jnp.where(behind < window[None, :], shifted, 0.0)
    sp_index = lax.axis_index("sp")
    position = sp_index * row_count + jnp.arange(row_count, dtype=jnp.int32)
    counted = jnp.minimum(position[:, None] + 1, window[None, :]).astype(jnp.float32)
    centered = (summed / counted - extended[reach:]).astype(jnp.bfloat16)
    pooled = jnp.einsum(
        "tgc,gcd->tgd",
        centered.reshape(row_count, local_groups, group_ch),
        pool_mix,
        preferred_element_type=jnp.float32,
    )
    pool_out = (pooled.reshape(row_count, pool_cols) * pool_scale).astype(jnp.bfloat16)
    score_scale = 1.0 / math.sqrt(HEAD_DIM)
    sp_count = lax.axis_size("sp")
    key_value = jnp.stack([key_heads, value_heads])
    everything = lax.all_gather(key_value, "sp", axis=1, tiled=True)
    half = row_count // 2
    bit_count = sp_count.bit_length() - 1

    def run_rows(query_rows, source, row_offset):
        start_carry = jnp.zeros((head_count, query_rows.shape[0]), jnp.float32)
        diagonal = lax.dynamic_slice_in_dim(everything, source * row_count, row_count, 1)
        first_out, first_carry = stick_block(
            query_rows, diagonal[0], diagonal[1], stick_offset, start_carry, row_offset, score_scale
        )

        def turn(turn_index, state):
            acc_out, acc_carry = state
            block = lax.dynamic_slice_in_dim(
                everything, (source - turn_index) * row_count, row_count, 1
            )
            block_out, block_total = stick_block(
                query_rows, block[0], block[1], stick_offset, acc_carry, None, score_scale
            )
            return (acc_out + block_out, acc_carry + block_total)

        result, unused = lax.fori_loop(1, source + 1, turn, (first_out, first_carry))
        return result.reshape(query_rows.shape[0], head_count * HEAD_DIM).astype(jnp.bfloat16)

    guest_query = query[half:]
    for bit in range(bit_count):
        guest_query = partner_2(guest_query, "sp", bit)
    partner = sp_count - 1 - sp_index
    own_rows = run_rows(query[:half], sp_index, 0)
    guest_rows = run_rows(guest_query, partner, half)
    for bit in range(bit_count):
        guest_rows = partner_2(guest_rows, "sp", bit)
    attn_out = jnp.concatenate([own_rows, guest_rows], axis=0)
    w_pool_cols, w_attn_cols = (
        lax.all_gather(w_out_pool, "fs", axis=1, tiled=True),
        lax.all_gather(w_out_attn, "fs", axis=1, tiled=True),
    )
    pool_rows, attn_rows = (
        lax.all_to_all(pool_out, "tp", split_axis=0, concat_axis=1, tiled=True),
        lax.all_to_all(attn_out, "tp", split_axis=0, concat_axis=1, tiled=True),
    )
    w_pool_all, w_attn_all, pool_gain_all, attn_gain_all = (
        lax.all_gather(w_pool_cols, "tp", axis=0, tiled=True),
        lax.all_gather(w_attn_cols, "tp", axis=0, tiled=True),
        lax.all_gather(pool_gain, "tp", axis=0, tiled=True),
        lax.all_gather(attn_gain, "tp", axis=0, tiled=True),
    )
    pool_f = pool_rows.astype(jnp.float32)
    attn_f = attn_rows.astype(jnp.float32)
    pool_normed = branch_norm(pool_rows, jnp.sum(pool_f * pool_f, axis=-1), POOL, pool_gain_all)
    attn_normed = branch_norm(
        attn_rows, jnp.sum(attn_f * attn_f, axis=-1), HEADS * HEAD_DIM, attn_gain_all
    )
    mixed = jnp.dot(pool_normed, w_pool_all, preferred_element_type=jnp.float32) + jnp.dot(
        attn_normed, w_attn_all, preferred_element_type=jnp.float32
    )
    return mixed.astype(jnp.bfloat16)[None]


def solution(mesh):
    in_specs = (
        P("fs", "sp", "tp"),
        P(),
        P("fs", "tp"),
        P("fs", "tp"),
        P("fs", "tp"),
        P("fs", "tp"),
        P(),
        P(),
        P("tp"),
        P("tp", None, None),
        P("tp"),
        P("tp"),
        P("tp"),
        P("tp", "fs"),
        P("tp", "fs"),
    )
    out_specs = P("fs", ("sp", "tp"), None)
    return jax.shard_map(shards, mesh=mesh, in_specs=in_specs, out_specs=out_specs, check_vma=False)
```

profile of v0, /device:TPU:103, one launch (start us, length us, event | category | flops | bytes accessed | tf_op | source)
XLA Modules:
  0.0 761.2 jit_solution(1497514801564157925)
XLA Ops:
  6.5 2.9 pad_maximum_fusion
  11.9 5.5 all-to-all-start
  20.0 3.0 copy.102
  27.3 57.7 %all-gather.9.cloned.1.call-done = bf16[2048,1792]{1,0:T(8,128)(2,1)} async-done(((bf16[512,1792]{1,0:T(8,128)(2,1)}), bf16[2048,1792]{1,0:T(8,128)(2,1)}) %all-gather.9.cloned.1.call-update) | async-done | bytes 7340048 | tf_op jit(solution)/shard_map/all_gather | solution.py:34
  85.0 3.9 slice_bitcast_fusion.5
  88.9 4.0 copy.106
  92.9 3.6 multiply_reduce_fusion.2
  96.8 3.0 fusion.82
  101.0 17.3 %all-gather.17.cloned.1.call-done = bf16[512,2048]{1,0:T(8,128)(2,1)} async-done(((bf16[512,512]{1,0:T(8,128)(2,1)}), bf16[512,2048]{1,0:T(8,128)(2,1)}) %all-gather.17.cloned.1.call-update) | async-done | bytes 2097168 | tf_op jit(solution)/shard_map/all_gather | solution.py:185
  121.2 3.6 multiply_reduce_fusion.1
  134.2 8.0 %all-gather.11.cloned.1.call-done = bf16[256,2048]{1,0:T(8,128)(2,1)} async-done(((bf16[256,512]{1,0:T(8,128)(2,1)}), bf16[256,2048]{1,0:T(8,128)(2,1)}) %all-gather.11.cloned.1.call-update) | async-done | bytes 1048592 | tf_op jit(solution)/shard_map/all_gather | solution.py:184
  146.6 6.6 all-to-all-start.1
  154.5 8.8 %collective-permute-done.3 = bf16[256,8,64]{0,2,1:T(8,128)(2,1)S(1)} collective-permute-done((bf16[256,8,64]{0,2,1:T(8,128)(2,1)S(1)}, bf16[256,8,64]{0,2,1:T(8,128)(2,1)S(1)}, u32[]{:S(2)}, u32[]{:S(2)}) %collective-permute-start.3) | collective-permute-done | bytes 262176 | tf_op jit(solution)/shard_map/ppermute | solution.py:48
  165.4 5.4 collective-permute-done.4
  170.8 97.9 %all-gather.15.cloned.1.call-done = bf16[2,8192,8,64]{1,3,2,0:T(8,128)(2,1)} async-done(((bf16[2,512,8,64]{1,3,2,0:T(8,128)(2,1)}), bf16[2,8192,8,64]{1,3,2,0:T(8,128)(2,1)}) %all-gather.15.cloned.1.call-update) | async-done | bytes 16777232 | tf_op jit(solution)/shard_map/all_gather | solution.py:150
  270.6 10.6 %fusion.63 = (f32[8,256,512]{2,1,0:T(8,128)}, f32[8,256,512]{2,1,0:T(8,128)}, f32[8,256,512]{2,1,0:T(8,128)}) fusion(f32[8]{0:T(128)S(1)} %copy-done.14, pred[256,512]{1,0:T(8,128)(4,1)S(1)} %get-tuple-element.157, f32[8,256,512]{2,1,0:T(8,128)S(1)} %fusion.97, pred[256,512]{1,0:T(8,128)(4,1)S(1)} %get-tuple-element.156, ...), kind=kOutput, calls=%fused_computation.79 | convolution fusion | flops 155189248 | bytes 17826308 | tf_op jit(solution)/shard_map/thd,khd->htk/dot_general | solution.py:59
  281.2 5.7 copy.122
  286.9 5.6 copy.124
  297.5 5.3 copy.125
  304.8 6.4 fusion.88
  311.4 14.4 %collective-permute-start.5 = (bf16[256,512]{0,1:T(8,128)(2,1)S(1)}, bf16[256,512]{0,1:T(8,128)(2,1)S(1)}, u32[]{:S(2)}, u32[]{:S(2)}) collective-permute-start(bf16[256,512]{0,1:T(8,128)(2,1)S(1)} %bitcast.254), channel_id=1, source_target_pairs={{0,8},{8,0},{16,24},{24,16},{32,40},{40,32},{48,56},{56,48},{64,72... | collective-permute-start | bytes 786440 | tf_op jit(solution)/shard_map/ppermute | solution.py:48
  330.5 28.5 %collective-permute-start.6 = (bf16[256,512]{0,1:T(8,128)(2,1)S(1)}, bf16[256,512]{0,1:T(8,128)(2,1)S(1)}, u32[]{:S(2)}, u32[]{:S(2)}) collective-permute-start(bf16[256,512]{0,1:T(8,128)(2,1)S(1)} %collective-permute-done.5), channel_id=1, source_target_pairs={{0,16},{8,24},{16,0},{24,8},{32,48},{40,56},{48,32},{56,40},{64,80... | collective-permute-start | bytes 786440 | tf_op jit(solution)/shard_map/ppermute | solution.py:48
  361.2 5.3 copy.123
  368.3 53.3 %collective-permute-start.7 = (bf16[256,512]{0,1:T(8,128)(2,1)S(1)}, bf16[256,512]{0,1:T(8,128)(2,1)S(1)}, u32[]{:S(2)}, u32[]{:S(2)}) collective-permute-start(bf16[256,512]{0,1:T(8,128)(2,1)S(1)} %collective-permute-done.6), channel_id=1, source_target_pairs={{0,32},{8,40},{16,48},{24,56},{32,0},{40,8},{48,16},{56,24},{64,96... | collective-permute-start | bytes 786440 | tf_op jit(solution)/shard_map/ppermute | solution.py:48
  421.7 6.4 fusion.85
  428.1 110.3 %collective-permute-start.8 = (bf16[256,512]{0,1:T(8,128)(2,1)S(1)}, bf16[256,512]{0,1:T(8,128)(2,1)S(1)}, u32[]{:S(2)}, u32[]{:S(2)}) collective-permute-start(bf16[256,512]{0,1:T(8,128)(2,1)S(1)} %collective-permute-done.7), channel_id=1, source_target_pairs={{0,64},{8,72},{16,80},{24,88},{32,96},{40,104},{48,112},{56,120},{... | collective-permute-start | bytes 786440 | tf_op jit(solution)/shard_map/ppermute | solution.py:48
  538.4 200.5 %while.24 = (s32[]{:T(128)}, f32[256,8,64]{0,2,1:T(8,128)S(1)}, f32[8,256]{1,0:T(8,128)S(1)}, s32[]{:T(128)}, s32[]{:T(128)}, /*index=5*/bf16[2,8192,8,64]{1,3,2...) while((s32[]{:T(128)}, f32[256,8,64]{0,2,1:T(8,128)S(1)}, ...), condition=%wide.region_9.10_spmd, body=%wide.region_6.9_spmd.sunk | while | flops 426934272 | bytes 44548372 | solution.py:171
  538.4 4.1 fusion.176
  542.5 2.6 fusion.177
  547.0 4.7 fusion.179
  551.8 4.1 fusion.176
  555.9 2.6 fusion.177
  560.4 4.7 fusion.179
  565.2 4.1 fusion.176
  573.7 4.7 fusion.179
  578.5 4.1 fusion.176
  587.1 4.7 fusion.179
  591.9 4.1 fusion.176
  596.0 2.6 fusion.177
  600.5 4.7 fusion.179
  605.3 4.1 fusion.176
  613.8 4.7 fusion.179
  618.6 4.1 fusion.176
  627.2 4.7 fusion.179
  632.0 4.1 fusion.176
  640.6 4.7 fusion.179
  645.4 4.1 fusion.176
  653.9 4.7 fusion.179
  658.7 4.1 fusion.176
  667.3 4.7 fusion.179
  672.1 4.1 fusion.176
  680.7 4.7 fusion.179
  685.5 4.1 fusion.176
  694.1 4.7 fusion.179
  698.8 4.1 fusion.176
  707.4 4.7 fusion.179
  712.2 4.1 fusion.176
  716.3 2.6 fusion.177
  720.8 4.7 fusion.179
  725.6 4.1 fusion.176
  734.2 4.7 fusion.179
  739.3 6.9 all_to_all.28
  747.1 3.5 fusion.138
  750.6 3.3 fusion.75
  (238 shorter events, 105.8 us)
Async XLA Ops:
  6.5 137.0 %copy-start = (bf16[2,128,128]{2,1,0:T(8,128)(2,1)S(1)}, bf16[2,128,128]{2,1,0:T(8,128)(2,1)}, u32[]{:S(2)}) copy-start(bf16[2,128,128]{2,1,0:T(8,128)(2,1)} %param.28) | copy-start | bytes 196612
  6.5 3.7 copy-start.5
  6.5 78.5 %all-gather.9.cloned.1.call-start = ((), (), s32[]{:S(2)}) async-start(), calls=%async_computation.3 | async-start | bytes 9175040 | tf_op jit(solution)/shard_map/all_gather | solution.py:34
  9.5 8.7 %copy-start.7 = (f32[2048]{0:T(1024)S(1)}, f32[2048]{0:T(1024)}, u32[]{:S(2)}) copy-start(f32[2048]{0:T(1024)} %param.20) | copy-start | bytes 24580
  9.5 108.8 %all-gather.17.cloned.1.call-start = ((), (), s32[]{:S(2)}) async-start(), calls=%async_computation.7 | async-start | bytes 2621440 | tf_op jit(solution)/shard_map/all_gather | solution.py:185
  11.9 8.1 %all-to-all-start = ((bf16[2,1,512,1024]{3,2,1,0:T(8,128)(2,1)}), bf16[2,1,512,1024]{3,2,1,0:T(8,128)(2,1)}, u32[]{:S(2)}, u32[]{:S(2)}) async-start(bf16[2,1,512,1024]{3,2,1,0:T(8,128)(2,1)} %broadcast_in_dim.182), calls=%async_computation | async-start | bytes 4194304 | tf_op jit(solution)/shard_map/all_to_all | solution.py:16
  17.4 124.8 %all-gather.11.cloned.1.call-start = ((), (), s32[]{:S(2)}) async-start(), calls=%async_computation.4 | async-start | bytes 1310720 | tf_op jit(solution)/shard_map/all_gather | solution.py:184
  18.1 250.7 %all-gather.15.cloned.1.call-start = ((), (), s32[]{:S(2)}) async-start(), calls=%async_computation.6 | async-start | bytes 17825792 | tf_op jit(solution)/shard_map/all_gather | solution.py:150
  92.9 3.7 copy-start.11
  92.9 3.9 copy-start.3
  100.9 646.2 %all-gather.19.cloned.1.call-start = ((), (), s32[]{:S(2)}) async-start(), calls=%async_computation.8 | async-start | bytes 6291456 | tf_op jit(solution)/shard_map/all_gather | solution.py:193
  118.3 632.3 %all-gather.13.cloned.1.call-start = ((), (), s32[]{:S(2)}) async-start(), calls=%async_computation.5 | async-start | bytes 3145728 | tf_op jit(solution)/shard_map/all_gather | solution.py:192
  121.2 3.7 copy-start.12
  121.2 4.6 copy-start.4
  124.9 4.3 copy-start.13
  124.9 6.9 copy-start.10
  125.2 17.1 %collective-permute-start.1 = (bf16[256,8,64]{0,2,1:T(8,128)(2,1)S(1)}, bf16[256,8,64]{0,2,1:T(8,128)(2,1)S(1)}, u32[]{:S(2)}, u32[]{:S(2)}) collective-permute-start(bf16[256,8,64]{0,2,1:T(8,128)(2,1)S(1)} %get-tuple-element.132), channel_id=1, source_target_pairs={{0,8},{8,0},{16,24},{24,16},{32,40},{40,32},{48,56},{56,48},{64,72... | collective-permute-start | bytes 786440 | tf_op jit(solution)/shard_map/ppermute | solution.py:48
  127.9 14.4 %collective-permute-start = (bf16[16,256]{1,0:T(8,128)(2,1)S(1)}, bf16[16,256]{1,0:T(8,128)(2,1)S(1)}, u32[]{:S(2)}, u32[]{:S(2)}) collective-permute-start(bf16[16,256]{1,0:T(8,128)(2,1)S(1)} %slice.170), channel_id=1, source_target_pairs={{0,8},{8,16},{16,24},{24,32},{32,40},{40,48},{48,56},{56,64},{64,7... | collective-permute-start | bytes 24584 | tf_op jit(solution)/shard_map/ppermute | solution.py:44
  142.3 10.9 %collective-permute-start.2 = (bf16[256,8,64]{0,2,1:T(8,128)(2,1)S(1)}, bf16[256,8,64]{0,2,1:T(8,128)(2,1)S(1)}, u32[]{:S(2)}, u32[]{:S(2)}) collective-permute-start(bf16[256,8,64]{0,2,1:T(8,128)(2,1)S(1)} %collective-permute-done.1), channel_id=1, source_target_pairs={{0,16},{8,24},{16,0},{24,8},{32,48},{40,56},{48,32},{56,40},{64,80... | collective-permute-start | bytes 786440 | tf_op jit(solution)/shard_map/ppermute | solution.py:48
  143.6 2.3 copy-start.9
  146.6 124.0 %copy-start.14 = (f32[8]{0:T(128)S(1)}, f32[8]{0:T(128)}, u32[]{:S(2)}) copy-start(f32[8]{0:T(128)} %param.27) | copy-start | bytes 100
  146.6 7.8 %all-to-all-start.1 = ((bf16[2,256,256]{2,1,0:T(8,128)(2,1)}), bf16[2,256,256]{2,1,0:T(8,128)(2,1)S(1)}, u32[]{:S(2)}, u32[]{:S(2)}) async-start(bf16[2,256,256]{2,1,0:T(8,128)(2,1)} %multiply_convert_fusion.3), calls=%async_computation.1 | async-start | bytes 524288 | tf_op jit(solution)/shard_map/all_to_all | solution.py:188
  153.2 10.2 %collective-permute-start.3 = (bf16[256,8,64]{0,2,1:T(8,128)(2,1)S(1)}, bf16[256,8,64]{0,2,1:T(8,128)(2,1)S(1)}, u32[]{:S(2)}, u32[]{:S(2)}) collective-permute-start(bf16[256,8,64]{0,2,1:T(8,128)(2,1)S(1)} %collective-permute-done.2), channel_id=1, source_target_pairs={{0,32},{8,40},{16,48},{24,56},{32,0},{40,8},{48,16},{56,24},{64,96... | collective-permute-start | bytes 786440 | tf_op jit(solution)/shard_map/ppermute | solution.py:48
  163.3 7.5 collective-permute-start.4
  270.6 10.6 %copy-start.2 = (f32[8,256,512]{2,1,0:T(8,128)}, f32[8,256,512]{2,1,0:T(8,128)S(1)}, u32[]{:S(2)}) copy-start(f32[8,256,512]{2,1,0:T(8,128)S(1)} %fusion.97) | copy-start | bytes 12582916
  311.4 19.1 %collective-permute-start.5 = (bf16[256,512]{0,1:T(8,128)(2,1)S(1)}, bf16[256,512]{0,1:T(8,128)(2,1)S(1)}, u32[]{:S(2)}, u32[]{:S(2)}) collective-permute-start(bf16[256,512]{0,1:T(8,128)(2,1)S(1)} %bitcast.254), channel_id=1, source_target_pairs={{0,8},{8,0},{16,24},{24,16},{32,40},{40,32},{48,56},{56,48},{64,72... | collective-permute-start | bytes 786440 | tf_op jit(solution)/shard_map/ppermute | solution.py:48
  330.5 37.8 %collective-permute-start.6 = (bf16[256,512]{0,1:T(8,128)(2,1)S(1)}, bf16[256,512]{0,1:T(8,128)(2,1)S(1)}, u32[]{:S(2)}, u32[]{:S(2)}) collective-permute-start(bf16[256,512]{0,1:T(8,128)(2,1)S(1)} %collective-permute-done.5), channel_id=1, source_target_pairs={{0,16},{8,24},{16,0},{24,8},{32,48},{40,56},{48,32},{56,40},{64,80... | collective-permute-start | bytes 786440 | tf_op jit(solution)/shard_map/ppermute | solution.py:48
  368.3 59.7 %collective-permute-start.7 = (bf16[256,512]{0,1:T(8,128)(2,1)S(1)}, bf16[256,512]{0,1:T(8,128)(2,1)S(1)}, u32[]{:S(2)}, u32[]{:S(2)}) collective-permute-start(bf16[256,512]{0,1:T(8,128)(2,1)S(1)} %collective-permute-done.6), channel_id=1, source_target_pairs={{0,32},{8,40},{16,48},{24,56},{32,0},{40,8},{48,16},{56,24},{64,96... | collective-permute-start | bytes 786440 | tf_op jit(solution)/shard_map/ppermute | solution.py:48
  428.1 310.9 %collective-permute-start.8 = (bf16[256,512]{0,1:T(8,128)(2,1)S(1)}, bf16[256,512]{0,1:T(8,128)(2,1)S(1)}, u32[]{:S(2)}, u32[]{:S(2)}) collective-permute-start(bf16[256,512]{0,1:T(8,128)(2,1)S(1)} %collective-permute-done.7), channel_id=1, source_target_pairs={{0,64},{8,72},{16,80},{24,88},{32,96},{40,104},{48,112},{56,120},{... | collective-permute-start | bytes 786440 | tf_op jit(solution)/shard_map/ppermute | solution.py:48
  738.9 7.9 %copy-start.8 = (f32[2,1,512]{2,1,0:T(1,128)S(1)}, f32[2,1,512]{2,1,0:T(1,128)}, u32[]{:S(2)}) copy-start(f32[2,1,512]{2,1,0:T(1,128)} %convert_element_type.154) | copy-start | bytes 12292
  746.9 3.8 copy-start.6
  747.1 6.8 copy-start.1
Sparse Core Ops, SparseCore 0:
  9.6 75.4 all-gather.8
  86.7 31.5 all-gather.16
  120.0 22.1 all-gather.10
  144.2 124.5 all-gather.14
  270.3 19.9 all-gather.18
  291.7 14.6 all-gather.12
where the time goes:
time: 772 us; the launch traced here: 761 us
  starting transfers between devices  224 us (29%)
  waiting for transfers between devices  201 us (26%)
  matrix products  178 us (23%)
  other arithmetic  68 us (9%)
  local copies, waits for them, and re-layouts  63.1 us (8%)
  between operations  14.4 us (2%)
  blocking collectives  11.4 us (1%)
    ppermute x8, starting transfers between devices, partner_2(): lax.ppermute(shard, axis, [(i, i ^ 1 << distance) for i in range(lax.axis...  210 us
    all_gather x1, waiting for transfers between devices, shards(): everything = lax.all_gather(key_value, 'sp', axis=1, tiled=True)  97.9 us
    dot_general x17, matrix products, stick_block(): jnp.einsum('htk,khd->thd', weight, value_heads, preferred_element_type=jn...  84 us
    dot_general x17, matrix products, stick_block(): jnp.einsum('thd,khd->htk', query, key_heads, preferred_element_type=jnp.f...  73.4 us
    another operation x52, other arithmetic  57.9 us
    all_gather x1, waiting for transfers between devices, in_one_piece(): whole, at, outs = (lax.all_gather(both, axis, axis=dim, tiled=True), 0, [])  57.7 us
    another operation x36, local copies, waits for them, and re-layouts  42.3 us
    all_gather x1, waiting for transfers between devices, shards(): lax.all_gather(w_out_attn, 'fs', axis=1, tiled=True)  17.3 us
  transfers between devices with their start and end apart: 17, of which 9 were waited for; matrix products, arithmetic and copies ran while one was open for 40% of the time, Pallas kernels for 0%

commit v1 on v0

--- a/solution.py
+++ b/solution.py
@@ -147,7 +147,9 @@
     score_scale = 1.0 / math.sqrt(HEAD_DIM)
     sp_count = lax.axis_size("sp")
     key_value = jnp.stack([key_heads, value_heads])
-    everything = lax.all_gather(key_value, "sp", axis=1, tiled=True)
+    everything = jnp.concatenate(
+        lax.all_to_all(jnp.stack([key_value] * lax.axis_size("sp")), "sp", 0, 0), axis=1
+    )
     half = row_count // 2
     bit_count = sp_count.bit_length() - 1
 

time: 772 us -> 908 us (1.18)
  waiting for transfers between devices: 201 us -> 314 us
  local copies, waits for them, and re-layouts: 63.1 us -> 79.7 us
  blocking collectives: 11.4 us -> 21.3 us
    ppermute x8, waiting for transfers between devices: 16.3 us -> 219 us  [partner_2(): lax.ppermute(shard, axis, [(i, i ^ 1 << distance) for i in range(lax.axis...]
    all_gather x1 -> x0, waiting for transfers between devices: 97.9 us -> none  [shards(): everything = lax.all_gather(key_value, 'sp', axis=1, tiled=True)]
    all_gather x1, waiting for transfers between devices: 17.3 us -> 32.7 us  [shards(): lax.all_gather(w_out_attn, 'fs', axis=1, tiled=True)]
    another operation x36 -> x37, local copies, waits for them, and re-layouts: 42.3 us -> 47.8 us
  transfers between devices with their start and end apart: 17 -> 16, of which waited for: 9 -> 7; matrix products, arithmetic and copies ran while one was open for 40% -> 33% of each run, Pallas kernels for 0% -> 0%
where the time goes in v1:
time: 908 us; the launch traced here: 897 us
  waiting for transfers between devices  314 us (35%)
  starting transfers between devices  222 us (24%)
  matrix products  176 us (19%)
  local copies, waits for them, and re-layouts  79.7 us (9%)
  other arithmetic  67.5 us (7%)
  blocking collectives  21.3 us (2%)
  between operations  14.1 us (2%)
    ppermute x8, waiting for transfers between devices, partner_2(): lax.ppermute(shard, axis, [(i, i ^ 1 << distance) for i in range(lax.axis...  219 us
    ppermute x8, starting transfers between devices, partner_2(): lax.ppermute(shard, axis, [(i, i ^ 1 << distance) for i in range(lax.axis...  208 us
    dot_general x17, matrix products, stick_block(): jnp.einsum('htk,khd->thd', weight, value_heads, preferred_element_type=jn...  84 us
    dot_general x17, matrix products, stick_block(): jnp.einsum('thd,khd->htk', query, key_heads, preferred_element_type=jnp.f...  71.8 us
    all_gather x1, waiting for transfers between devices, in_one_piece(): whole, at, outs = (lax.all_gather(both, axis, axis=dim, tiled=True), 0, [])  58.3 us
    another operation x52, other arithmetic  57.8 us
    another operation x36, local copies, waits for them, and re-layouts  41.9 us
    all_gather x1, waiting for transfers between devices, shards(): lax.all_gather(w_out_attn, 'fs', axis=1, tiled=True)  32.7 us
  transfers between devices with their start and end apart: 16, of which 7 were waited for; matrix products, arithmetic and copies ran while one was open for 33% of the time, Pallas kernels for 0%

profile of v1, /device:TPU:103, one launch (start us, length us, event | category | flops | bytes accessed | tf_op | source)
XLA Modules:
  0.0 896.5 jit_solution(2354935361996138953)
XLA Ops:
  6.5 3.0 pad_maximum_fusion
  11.1 5.5 all-to-all-start
  16.7 2.6 all-to-all-done
  19.3 3.0 copy.103
  26.8 58.3 %all-gather.8.cloned.1.call-done = bf16[2048,1792]{1,0:T(8,128)(2,1)} async-done(((bf16[512,1792]{1,0:T(8,128)(2,1)}), bf16[2048,1792]{1,0:T(8,128)(2,1)}) %all-gather.8.cloned.1.call-update) | async-done | bytes 7340048 | tf_op jit(solution)/shard_map/all_gather | solution.py:34
  85.1 3.8 slice_bitcast_fusion.5
  88.9 3.9 copy.107
  92.9 3.6 multiply_reduce_fusion.2
  100.1 2.9 fusion.82
  109.1 5.4 all_to_all.33
  114.5 6.0 stack.8
  120.5 7.4 all-to-all-start.2
  129.4 32.7 %all-gather.14.cloned.1.call-done = bf16[512,2048]{1,0:T(8,128)(2,1)} async-done(((bf16[512,512]{1,0:T(8,128)(2,1)}), bf16[512,2048]{1,0:T(8,128)(2,1)}) %all-gather.14.cloned.1.call-update) | async-done | bytes 2097168 | tf_op jit(solution)/shard_map/all_gather | solution.py:187
  164.7 3.5 multiply_reduce_fusion.1
  169.2 210.3 %collective-permute-done.1 = bf16[256,8,64]{0,2,1:T(8,128)(2,1)S(1)} collective-permute-done((bf16[256,8,64]{0,2,1:T(8,128)(2,1)S(1)}, bf16[256,8,64]{0,2,1:T(8,128)(2,1)S(1)}, u32[]{:S(2)}, u32[]{:S(2)}) %collective-permute-start.1) | collective-permute-done | bytes 262176 | tf_op jit(solution)/shard_map/ppermute | solution.py:48
  380.0 2.9 all-gather
  388.1 5.4 collective-permute-done.3
  396.1 8.8 copy.131
  405.7 10.0 %fusion.63 = (f32[8,256,512]{2,1,0:T(8,128)}, f32[8,256,512]{2,1,0:T(8,128)}, f32[8,256,512]{2,1,0:T(8,128)}) fusion(f32[8]{0:T(128)S(1)} %copy-done.14, pred[256,512]{1,0:T(8,128)(4,1)S(1)} %get-tuple-element.157, f32[8,256,512]{2,1,0:T(8,128)S(1)} %fusion.97, pred[256,512]{1,0:T(8,128)(4,1)S(1)} %get-tuple-element.156, ...), kind=kOutput, calls=%fused_computation.79 | convolution fusion | flops 155189248 | bytes 17826308 | tf_op jit(solution)/shard_map/thd,khd->htk/dot_general | solution.py:59
  415.7 5.5 copy.124
  421.2 5.5 copy.126
  431.6 5.3 copy.127
  438.7 6.4 fusion.88
  445.4 12.7 %collective-permute-start.5 = (bf16[256,512]{0,1:T(8,128)(2,1)S(1)}, bf16[256,512]{0,1:T(8,128)(2,1)S(1)}, u32[]{:S(2)}, u32[]{:S(2)}) collective-permute-start(bf16[256,512]{0,1:T(8,128)(2,1)S(1)} %bitcast.261), channel_id=1, source_target_pairs={{0,8},{8,0},{16,24},{24,16},{32,40},{40,32},{48,56},{56,48},{64,72... | collective-permute-start | bytes 786440 | tf_op jit(solution)/shard_map/ppermute | solution.py:48
  461.9 29.6 %collective-permute-start.6 = (bf16[256,512]{0,1:T(8,128)(2,1)S(1)}, bf16[256,512]{0,1:T(8,128)(2,1)S(1)}, u32[]{:S(2)}, u32[]{:S(2)}) collective-permute-start(bf16[256,512]{0,1:T(8,128)(2,1)S(1)} %collective-permute-done.5), channel_id=1, source_target_pairs={{0,16},{8,24},{16,0},{24,8},{32,48},{40,56},{48,32},{56,40},{64,80... | collective-permute-start | bytes 786440 | tf_op jit(solution)/shard_map/ppermute | solution.py:48
  493.8 5.3 copy.125
  500.9 52.9 %collective-permute-start.7 = (bf16[256,512]{0,1:T(8,128)(2,1)S(1)}, bf16[256,512]{0,1:T(8,128)(2,1)S(1)}, u32[]{:S(2)}, u32[]{:S(2)}) collective-permute-start(bf16[256,512]{0,1:T(8,128)(2,1)S(1)} %collective-permute-done.6), channel_id=1, source_target_pairs={{0,32},{8,40},{16,48},{24,56},{32,0},{40,8},{48,16},{56,24},{64,96... | collective-permute-start | bytes 786440 | tf_op jit(solution)/shard_map/ppermute | solution.py:48
  553.9 6.4 fusion.85
  560.3 109.6 %collective-permute-start.8 = (bf16[256,512]{0,1:T(8,128)(2,1)S(1)}, bf16[256,512]{0,1:T(8,128)(2,1)S(1)}, u32[]{:S(2)}, u32[]{:S(2)}) collective-permute-start(bf16[256,512]{0,1:T(8,128)(2,1)S(1)} %collective-permute-done.7), channel_id=1, source_target_pairs={{0,64},{8,72},{16,80},{24,88},{32,96},{40,104},{48,112},{56,120},{... | collective-permute-start | bytes 786440 | tf_op jit(solution)/shard_map/ppermute | solution.py:48
  669.9 200.5 %while.24 = (s32[]{:T(128)}, f32[256,8,64]{0,2,1:T(8,128)S(1)}, f32[8,256]{1,0:T(8,128)S(1)}, s32[]{:T(128)}, s32[]{:T(128)}, /*index=5*/bf16[2,8192,8,64]{1,3,2...) while((s32[]{:T(128)}, f32[256,8,64]{0,2,1:T(8,128)S(1)}, ...), condition=%wide.region_9.10_spmd, body=%wide.region_6.9_spmd.sunk | while | flops 426934272 | bytes 44548372 | solution.py:173
  669.9 4.1 fusion.176
  674.0 2.6 fusion.177
  678.5 4.7 fusion.179
  683.3 4.1 fusion.176
  691.9 4.7 fusion.179
  696.7 4.1 fusion.176
  705.2 4.7 fusion.179
  710.0 4.1 fusion.176
  718.6 4.7 fusion.179
  723.4 4.1 fusion.176
  732.0 4.7 fusion.179
  736.8 4.1 fusion.176
  745.3 4.7 fusion.179
  750.1 4.1 fusion.176
  758.7 4.7 fusion.179
  763.5 4.1 fusion.176
  772.1 4.7 fusion.179
  776.9 4.1 fusion.176
  785.4 4.7 fusion.179
  790.2 4.1 fusion.176
  798.8 4.7 fusion.179
  803.6 4.1 fusion.176
  812.2 4.7 fusion.179
  817.0 4.1 fusion.176
  825.5 4.7 fusion.179
  830.3 4.1 fusion.176
  838.9 4.7 fusion.179
  843.7 4.1 fusion.176
  852.3 4.7 fusion.179
  857.1 4.1 fusion.176
  865.6 4.7 fusion.179
  870.7 11.2 %all_to_all.34 = bf16[2,256,512]{2,1,0:T(8,128)(2,1)S(1)} all-to-all(bf16[2,256,512]{2,1,0:T(8,128)(2,1)S(1)} %bitcast.255), channel_id=1, replica_groups=mesh['sp'=16,'fs'=4,'tp'=2] {'tp'}, dimensions={0} | all-to-all | bytes 1048576 | tf_op jit(solution)/shard_map/all_to_all | solution.py:191
  882.8 3.5 fusion.138
  886.3 3.3 fusion.75
  (238 shorter events, 109.8 us)
Async XLA Ops:
  6.5 96.6 %copy-start = (bf16[2,128,128]{2,1,0:T(8,128)(2,1)S(1)}, bf16[2,128,128]{2,1,0:T(8,128)(2,1)}, u32[]{:S(2)}) copy-start(bf16[2,128,128]{2,1,0:T(8,128)(2,1)} %param.28) | copy-start | bytes 196612
  6.5 3.0 copy-start.5
  6.5 78.6 %all-gather.8.cloned.1.call-start = ((), (), s32[]{:S(2)}) async-start(), calls=%async_computation.4 | async-start | bytes 9175040 | tf_op jit(solution)/shard_map/all_gather | solution.py:34
  9.5 7.2 copy-start.7
  11.1 8.2 all-to-all-start
  92.9 3.7 copy-start.4
  96.5 3.3 copy-start.11
  98.5 4.5 collective-permute-start
  103.1 4.9 copy-start.9
  120.5 275.6 %all-to-all-start.2 = ((bf16[16,2,512,8,64]{2,4,3,1,0:T(8,128)(2,1)}), bf16[16,2,512,8,64]{2,4,3,1,0:T(8,128)(2,1)}, u32[]{:S(2)}, u32[]{:S(2)}) async-start(bf16[16,2,512,8,64]{2,4,3,1,0:T(8,128)(2,1)} %stack.8), calls=%async_computation.2 | async-start | bytes 33554432 | tf_op jit(solution)/shard_map/all_to_all | solution.py:151
  127.9 34.3 %all-gather.14.cloned.1.call-start = ((), (), s32[]{:S(2)}) async-start(), calls=%async_computation.7 | async-start | bytes 2621440 | tf_op jit(solution)/shard_map/all_gather | solution.py:187
  128.6 257.0 %all-gather.10.cloned.1.call-start = ((), (), s32[]{:S(2)}) async-start(), calls=%async_computation.5 | async-start | bytes 1310720 | tf_op jit(solution)/shard_map/all_gather | solution.py:186
  129.4 753.4 %all-gather.16.cloned.1.call-start = ((), (), s32[]{:S(2)}) async-start(), calls=%async_computation.8 | async-start | bytes 6291456 | tf_op jit(solution)/shard_map/all_gather | solution.py:195
  162.2 724.2 %all-gather.12.cloned.1.call-start = ((), (), s32[]{:S(2)}) async-start(), calls=%async_computation.6 | async-start | bytes 3145728 | tf_op jit(solution)/shard_map/all_gather | solution.py:194
  164.7 3.5 copy-start.12
  164.7 215.3 %copy-start.13 = (bf16[256]{0:T(256)(128)(2,1)S(1)}, bf16[256]{0:T(256)(128)(2,1)}, u32[]{:S(2)}) copy-start(bf16[256]{0:T(256)(128)(2,1)} %param.30) | copy-start | bytes 1540
  164.7 218.2 %copy-start.10 = (bf16[512]{0:T(512)(128)(2,1)S(1)}, bf16[512]{0:T(512)(128)(2,1)}, u32[]{:S(2)}) copy-start(bf16[512]{0:T(512)(128)(2,1)} %param.31) | copy-start | bytes 3076
  168.5 211.0 %collective-permute-start.1 = (bf16[256,8,64]{0,2,1:T(8,128)(2,1)S(1)}, bf16[256,8,64]{0,2,1:T(8,128)(2,1)S(1)}, u32[]{:S(2)}, u32[]{:S(2)}) collective-permute-start(bf16[256,8,64]{0,2,1:T(8,128)(2,1)S(1)} %get-tuple-element.132), channel_id=1, source_target_pairs={{0,8},{8,0},{16,24},{24,16},{32,40},{40,32},{48,56},{56,48},{64,72... | collective-permute-start | bytes 786440 | tf_op jit(solution)/shard_map/ppermute | solution.py:48
  379.5 8.4 collective-permute-start.2
  387.9 5.6 collective-permute-start.3
  393.4 11.5 %collective-permute-start.4 = (bf16[256,8,64]{0,2,1:T(8,128)(2,1)S(1)}, bf16[256,8,64]{0,2,1:T(8,128)(2,1)S(1)}, u32[]{:S(2)}, u32[]{:S(2)}) collective-permute-start(bf16[256,8,64]{0,2,1:T(8,128)(2,1)S(1)} %collective-permute-done.3), channel_id=1, source_target_pairs={{0,64},{8,72},{16,80},{24,88},{32,96},{40,104},{48,112},{56,120},{... | collective-permute-start | bytes 786440 | tf_op jit(solution)/shard_map/ppermute | solution.py:48
  404.9 10.8 %copy-start.2 = (bf16[16,2,8,8,8,512]{5,4,0,3,2,1:T(8,128)(2,1)}, bf16[16,2,8,8,8,512]{5,4,0,3,2,1:T(8,128)(2,1)S(1)}, u32[]{:S(2)}) copy-start(bf16[16,2,8,8,8,512]{5,4,0,3,2,1:T(8,128)(2,1)S(1)} %copy.131) | copy-start | bytes 50331652
  404.9 0.8 copy-start.14
  405.7 10.1 %copy-start.3 = (f32[8,256,512]{2,1,0:T(8,128)}, f32[8,256,512]{2,1,0:T(8,128)S(1)}, u32[]{:S(2)}) copy-start(f32[8,256,512]{2,1,0:T(8,128)S(1)} %fusion.97) | copy-start | bytes 12582916
  445.4 16.5 %collective-permute-start.5 = (bf16[256,512]{0,1:T(8,128)(2,1)S(1)}, bf16[256,512]{0,1:T(8,128)(2,1)S(1)}, u32[]{:S(2)}, u32[]{:S(2)}) collective-permute-start(bf16[256,512]{0,1:T(8,128)(2,1)S(1)} %bitcast.261), channel_id=1, source_target_pairs={{0,8},{8,0},{16,24},{24,16},{32,40},{40,32},{48,56},{56,48},{64,72... | collective-permute-start | bytes 786440 | tf_op jit(solution)/shard_map/ppermute | solution.py:48
  461.9 39.0 %collective-permute-start.6 = (bf16[256,512]{0,1:T(8,128)(2,1)S(1)}, bf16[256,512]{0,1:T(8,128)(2,1)S(1)}, u32[]{:S(2)}, u32[]{:S(2)}) collective-permute-start(bf16[256,512]{0,1:T(8,128)(2,1)S(1)} %collective-permute-done.5), channel_id=1, source_target_pairs={{0,16},{8,24},{16,0},{24,8},{32,48},{40,56},{48,32},{56,40},{64,80... | collective-permute-start | bytes 786440 | tf_op jit(solution)/shard_map/ppermute | solution.py:48
  500.9 59.4 %collective-permute-start.7 = (bf16[256,512]{0,1:T(8,128)(2,1)S(1)}, bf16[256,512]{0,1:T(8,128)(2,1)S(1)}, u32[]{:S(2)}, u32[]{:S(2)}) collective-permute-start(bf16[256,512]{0,1:T(8,128)(2,1)S(1)} %collective-permute-done.6), channel_id=1, source_target_pairs={{0,32},{8,40},{16,48},{24,56},{32,0},{40,8},{48,16},{56,24},{64,96... | collective-permute-start | bytes 786440 | tf_op jit(solution)/shard_map/ppermute | solution.py:48
  560.3 310.2 %collective-permute-start.8 = (bf16[256,512]{0,1:T(8,128)(2,1)S(1)}, bf16[256,512]{0,1:T(8,128)(2,1)S(1)}, u32[]{:S(2)}, u32[]{:S(2)}) collective-permute-start(bf16[256,512]{0,1:T(8,128)(2,1)S(1)} %collective-permute-done.7), channel_id=1, source_target_pairs={{0,64},{8,72},{16,80},{24,88},{32,96},{40,104},{48,112},{56,120},{... | collective-permute-start | bytes 786440 | tf_op jit(solution)/shard_map/ppermute | solution.py:48
  870.4 12.1 %copy-start.8 = (f32[2,1,512]{2,1,0:T(1,128)S(1)}, f32[2,1,512]{2,1,0:T(1,128)}, u32[]{:S(2)}) copy-start(f32[2,1,512]{2,1,0:T(1,128)} %convert_element_type.154) | copy-start | bytes 12292
  882.6 3.8 copy-start.6
  882.8 6.8 copy-start.1
Sparse Core Ops, SparseCore 0:
  9.7 75.4 all-gather.7
  130.3 31.7 all-gather.13
  163.8 22.4 all-gather.9
  187.8 19.0 all-gather.15
  385.7 14.9 all-gather.11
